TPU v7x, 32 devices: a whole 2x2x4 slice. The times are simulated.
32 devices in a mesh: ep: 8 (over z, x), tp: 4 (over y, core).
Axes of the slice: x: 2, y: 2, z: 4, core: 2. Of those that a mesh axis runs over, the one named last changes fastest.
Arguments:
- mixer_input: bfloat16 [5120, 2048], P('ep'), may hold values from -6 to 6
- mixer_gain: float32 [2048], replicated, may hold values from 0.1 to 1.9
- value_weight: bfloat16 [2048, 1024], P(None, 'tp'), may hold values from -0.125 to 0.125
- inner_gate: bfloat16 [2048, 1024], P(None, 'tp'), may hold values from -0.125 to 0.125
- outer_gate: bfloat16 [2048, 1024], P(None, 'tp'), may hold values from -0.125 to 0.125
- kernel_taps: float32 [3, 1024], P(None, 'tp'), may hold values from -3 to 3
- mixer_proj: bfloat16 [1024, 2048], P('tp'), may hold values from -0.1875 to 0.1875
- expert_input: bfloat16 [5120, 2048], P(('ep', 'tp')), may hold values from -6 to 6
- expert_gain: float32 [2048], replicated, may hold values from 0.1 to 1.9
- routes: int32 [5120, 2], P(('ep', 'tp')), may hold values from 0 to 7, as said below
- group_logits: float32 [5120, 1], P(('ep', 'tp')), may hold values from -6 to 6
- pair_logits: float32 [5120, 2], P(('ep', 'tp')), may hold values from -6 to 6
- gate_weight: bfloat16 [8, 2048, 1024], P('ep', None, 'tp'), may hold values from -0.125 to 0.125
- up_weight: bfloat16 [8, 2048, 1024], P('ep', None, 'tp'), may hold values from -0.125 to 0.125
- down_weight: bfloat16 [8, 1024, 2048], P('ep', 'tp'), may hold values from -0.75 to 0.75
Outputs:
- mixer_output: bfloat16 [5120, 2048], P(('ep', 'tp'))
- expert_output: bfloat16 [5120, 2048], P(('ep', 'tp'))
Inputs may be any that keep to these rules, and one draw needn't show every extreme that they name: `routes`: both entries of a row are different experts of one group (equal after integer division by 8). In the rows of one device every group is chosen by the same number of rows, no expert is named more than 80 times, and in every draw one expert is named exactly 80 times in the rows of every device.
All inputs are finite; a program needn't handle non-finite values.
Results may differ from a plain program's by a relative error of at most 0.01.
Values may be sent and summed in bfloat16 or wider, within the bound.
A program may use at most 128 MiB of HBM per device.

v0:
```python
import jax
import jax.numpy as jnp
from jax import lax
from jax.sharding import PartitionSpec as P

EPG = 8
EPSILON = 1e-06


def padded_2(cells, sides, width):
    for axis, dim in sides:
        count = lax.axis_size(axis)
        ends = count - 1
        head = lax.slice_in_dim(cells, 0, width, axis=dim)
        tail = lax.slice_in_dim(cells, cells.shape[dim] - width, cells.shape[dim], axis=dim)
        cells = jnp.concatenate(
            [
                lax.ppermute(tail, axis, [(i, (i + 1) % count) for i in range(ends)]),
                cells,
                lax.ppermute(head, axis, [((i + 1) % count, i) for i in range(ends)]),
            ],
            axis=dim,
        )
    return cells


def normed(values, gain):
    wide = values.astype(jnp.float32)
    scale = lax.rsqrt(jnp.mean(wide * wide, axis=-1, keepdims=True) + EPSILON)
    return (wide * scale * gain).astype(jnp.bfloat16)


def blockwise_sum(left, right, blocks):
    width = left.shape[1] // blocks
    total = jnp.zeros((left.shape[0], right.shape[1]), jnp.float32)
    for block in range(blocks):
        part = jnp.dot(
            left[:, block * width : (block + 1) * width],
            right[block * width : (block + 1) * width],
            preferred_element_type=jnp.float32,
        )
        rounded = lax.optimization_barrier(part.astype(jnp.bfloat16))
        total = total + rounded.astype(jnp.float32)
    return total.astype(jnp.bfloat16)


def route_weights(routes, group_logits, pair_logits):
    chosen = routes[:, 0] // EPG
    groups = jnp.arange(group_logits.shape[1], dtype=jnp.int32)
    picked = jnp.sum(jnp.where(groups[None, :] == chosen[:, None], group_logits, 0.0), axis=1)
    group_weight = 1.0 / jnp.sum(jnp.exp(group_logits - picked[:, None]), axis=1)
    return group_weight[:, None] * jax.nn.sigmoid(pair_logits - pair_logits[:, ::-1])


def on_device(
    mixer_input,
    mixer_gain,
    value_weight,
    inner_gate,
    outer_gate,
    kernel_taps,
    mixer_proj,
    expert_input,
    expert_gain,
    routes,
    group_logits,
    pair_logits,
    gate_weight,
    up_weight,
    down_weight,
):
    split = lax.axis_size("tp")
    normal_rows = normed(mixer_input, mixer_gain)
    values = jnp.dot(normal_rows, value_weight, preferred_element_type=jnp.float32)
    inner = jnp.dot(normal_rows, inner_gate, preferred_element_type=jnp.float32)
    outer = jnp.dot(normal_rows, outer_gate, preferred_element_type=jnp.float32)
    mixed_in = (inner * values).astype(jnp.bfloat16)
    padded = padded_2(mixed_in, (("ep", 0),), 1).astype(jnp.float32)
    conv_sum = (
        kernel_taps[0] * padded[:-2] + kernel_taps[1] * padded[1:-1] + kernel_taps[2] * padded[2:]
    )
    mixer_rows = (outer * conv_sum).astype(jnp.bfloat16)
    mixer_output = lax.psum_scatter(
        jnp.dot(mixer_rows, mixer_proj, preferred_element_type=jnp.float32).astype(jnp.bfloat16),
        "tp",
        scatter_dimension=0,
        tiled=True,
    )
    expert_norm = normed(expert_input, expert_gain)
    weights = route_weights(routes, group_logits, pair_logits)
    experts = lax.axis_size("ep")
    local = expert_norm.shape[0]
    width = expert_norm.shape[1]
    capacity = 4 * local // experts
    flat = routes.reshape(-1)
    onehot = (flat[:, None] == jnp.arange(experts, dtype=jnp.int32)[None, :]).astype(jnp.int32)
    before = jnp.sum((jnp.cumsum(onehot, axis=0) - onehot) * onehot, axis=1)
    slots = flat * capacity + before
    sources = (
        jnp.full((experts * capacity,), local, jnp.int32)
        .at[slots]
        .set(jnp.arange(2 * local, dtype=jnp.int32) // 2)
    )
    rows_pad = jnp.concatenate([expert_norm, jnp.zeros((1, width), jnp.bfloat16)])
    outgoing = rows_pad[sources].reshape(experts, capacity, width)
    whole_gate, whole_up, whole_down = (
        lax.all_gather(gate_weight, "tp", axis=2, tiled=True),
        lax.all_gather(up_weight, "tp", axis=2, tiled=True),
        lax.all_gather(down_weight, "tp", axis=1, tiled=True),
    )
    arrived = lax.all_to_all(outgoing, "ep", split_axis=0, concat_axis=0, tiled=True)
    senders, items, _ = arrived.shape
    answers = expert_block_local(
        arrived.reshape(senders * items, width), whole_gate[0], whole_up[0], whole_down[0], split
    )
    returned = lax.all_to_all(
        answers.reshape(senders, items, width), "ep", split_axis=0, concat_axis=0, tiled=True
    )
    answered = returned.reshape(experts * capacity, width)
    pairs = answered[slots].reshape(local, 2, width)
    expert_output = (
        weights[:, 0:1] * pairs[:, 0].astype(jnp.float32)
        + weights[:, 1:2] * pairs[:, 1].astype(jnp.float32)
    ).astype(jnp.bfloat16)
    return (mixer_output, expert_output)


def expert_block_local(rows, gate, upper, down, blocks):
    first = jnp.dot(rows, gate, preferred_element_type=jnp.float32)
    second = jnp.dot(rows, upper, preferred_element_type=jnp.float32)
    hidden = (jax.nn.silu(first) * second).astype(jnp.bfloat16)
    return blockwise_sum(hidden, down, blocks)


def solution(mesh):
    in_specs = (
        P("ep", None),
        P(),
        P(None, "tp"),
        P(None, "tp"),
        P(None, "tp"),
        P(None, "tp"),
        P("tp", None),
        P(("ep", "tp"), None),
        P(),
        P(("ep", "tp"), None),
        P(("ep", "tp"), None),
        P(("ep", "tp"), None),
        P("ep", None, "tp"),
        P("ep", None, "tp"),
        P("ep", "tp", None),
    )
    out_specs = (P(("ep", "tp"), None), P(("ep", "tp"), None))
    return jax.shard_map(
        on_device, mesh=mesh, in_specs=in_specs, out_specs=out_specs, check_vma=False
    )
```

profile of v0, /device:TPU:0, one launch (start us, length us, event | category | flops | bytes accessed | tf_op | source)
XLA Modules:
  0.0 216.1 jit_solution(17580793458356525415)
XLA Ops:
  9.6 0.9 reduce-window.6
  12.4 2.9 %scatter_custom_fusion = s32[640]{0:T(1024)S(1)} fusion(s32[320]{0:T(512)S(1)} %fusion.34, s32[320]{0:T(512)S(1)} %add_select_fusion, s32[]{:T(128)} %constant.59.clone.1), kind=kCustom, calls=%fused_computation.75 | custom fusion | bytes 2564 | tf_op jit(solution)/shard_map/scatter | solution.py:102
  15.3 4.1 %gather_fusion = bf16[640,2048]{1,0:T(8,128)(2,1)} fusion(bf16[161,2048]{1,0:T(8,128)(2,1)S(1)} %concatenate.7, s32[1024]{0:T(1024)S(1)} %pad_clamp_fusion.1), kind=kCustom, calls=%fused_computation | custom fusion | bytes 5245440 | tf_op jit(solution)/shard_map/gather | solution.py:105
  19.4 7.3 %all-to-all-start = ((bf16[8,80,2048]{2,1,0:T(8,128)(2,1)}), bf16[8,80,2048]{2,1,0:T(8,128)(2,1)}, u32[]{:S(2)}, u32[]{:S(2)}) async-start(bf16[8,80,2048]{2,1,0:T(8,128)(2,1)} %bitcast.53), calls=%async_computation.1 | async-start | bytes 5242880 | tf_op jit(solution)/shard_map/all_to_all | solution.py:111
  27.4 2.5 %fusion = f32[640]{0:T(1024)S(1)} fusion(bf16[640,2048]{1,0:T(8,128)(2,1)} %param.15), kind=kLoop, calls=%fused_computation.5 | loop fusion | flops 3931520 | bytes 2624000 | tf_op jit(solution)/shard_map/reduce_sum | solution.py:29
  30.0 0.9 fusion.37
  31.3 0.9 fusion.15
  32.2 3.9 %collective-permute-start = (bf16[1,256]{1,0:T(2,128)(2,1)S(1)}, bf16[1,256]{1,0:T(2,128)(2,1)S(1)}, u32[]{:S(2)}, u32[]{:S(2)}) collective-permute-start(bf16[1,256]{1,0:T(2,128)(2,1)S(1)} %get-tuple-element.4), channel_id=1, source_target_pairs={{0,4},{4,8},{8,12},{12,16},{16,20},{20,24},{24,28},{1,5},{5,9},{9,... | collective-permute-start | bytes 1544 | tf_op jit(solution)/shard_map/ppermute | solution.py:18
  36.1 1.5 collective-permute-start.1
  37.6 10.4 %collective-permute-done = bf16[1,256]{1,0:T(2,128)(2,1)S(1)} collective-permute-done((bf16[1,256]{1,0:T(2,128)(2,1)S(1)}, bf16[1,256]{1,0:T(2,128)(2,1)S(1)}, u32[]{:S(2)}, u32[]{:S(2)}) %collective-permute-start) | collective-permute-done | bytes 544 | tf_op jit(solution)/shard_map/ppermute | solution.py:18
  48.2 38.1 %all-to-all-done = bf16[8,80,2048]{2,1,0:T(8,128)(2,1)} async-done(((bf16[8,80,2048]{2,1,0:T(8,128)(2,1)}), bf16[8,80,2048]{2,1,0:T(8,128)(2,1)}, u32[]{:S(2)}, u32[]{:S(2)}) %all-to-all-start) | async-done | bytes 2621472 | tf_op jit(solution)/shard_map/all_to_all | solution.py:111
  86.3 7.3 %fusion.3 = f32[640,1024]{1,0:T(8,128)} fusion(bf16[640,2048]{1,0:T(8,128)(2,1)} %bitcast.9, bf16[1,2048,1024]{2,1,0:T(8,128)(2,1)} %all-gather.6.cloned.1.call-done), kind=kOutput, calls=%fused_computation.9 | convolution fusion | flops 2684354560 | bytes 9437184 | tf_op jit(solution)/shard_map/dot_general | solution.py:130
  93.6 7.5 %multiply_convert_fusion = bf16[640,1024]{1,0:T(8,128)(2,1)S(1)} fusion(f32[640,1024]{1,0:T(8,128)} %fusion.3, bf16[640,2048]{1,0:T(8,128)(2,1)} %bitcast.9, bf16[1,2048,1024]{2,1,0:T(8,128)(2,1)} %all-gather.4.cloned.1.call-done), kind=kOutput, calls=%fused_computation.18 | convolution fusion | flops 2688286720 | bytes 10747904 | tf_op jit(solution)/shard_map/dot_general | solution.py:129
  101.1 18.9 %all-gather.8.cloned.1.call-done = bf16[1,1024,2048]{2,1,0:T(8,128)(2,1)} async-done(((bf16[1,256,2048]{2,1,0:T(8,128)(2,1)}), bf16[1,1024,2048]{2,1,0:T(8,128)(2,1)}) %all-gather.8.cloned.1.call-update) | async-done | bytes 4194320 | tf_op jit(solution)/shard_map/all_gather | solution.py:109
  120.0 2.2 %convolution_convert_fusion.3 = bf16[640,2048]{1,0:T(8,128)(2,1)S(1)} fusion(bf16[1,1024,2048]{2,1,0:T(8,128)(2,1)} %all-gather.8.cloned.1.call-done, bf16[640,1024]{1,0:T(8,128)(2,1)S(1)} %multiply_convert_fusion), kind=kOutput, calls=%fused_computation.16 | convolution fusion | flops 672399360 | bytes 3997696 | tf_op jit(solution)/shard_map/dot_general | solution.py:37
  122.2 2.1 convolution_convert_fusion.2
  126.0 3.8 %add_convert_fusion = bf16[640,2048]{1,0:T(8,128)(2,1)} fusion(bf16[640,2048]{1,0:T(8,128)(2,1)S(1)} %convolution_convert_fusion, bf16[640,2048]{1,0:T(8,128)(2,1)S(1)} %convolution_convert_fusion.1, bf16[640,2048]{1,0:T(8,128)(2,1)S(1)} %convolution_convert_fusion.2, bf16[640,2048]{1,0:T(8,128)(2,1)S(1)} %convolution_convert_fusion.3), kind=kLoop, calls=%fused_computation.8 | loop fusion | flops 10485760 | bytes 13107200 | tf_op jit(solution)/shard_map/convert_element_type | solution.py:44
  129.9 5.6 %all-to-all-start.1 = ((bf16[8,80,2048]{2,1,0:T(8,128)(2,1)}), bf16[8,80,2048]{2,1,0:T(8,128)(2,1)}, u32[]{:S(2)}, u32[]{:S(2)}) async-start(bf16[8,80,2048]{2,1,0:T(8,128)(2,1)} %bitcast.54), calls=%async_computation.2 | async-start | bytes 5242880 | tf_op jit(solution)/shard_map/all_to_all | solution.py:116
  135.8 6.1 %convolution_convert_fusion.4 = bf16[640,2048]{1,0:T(8,128)(2,1)} fusion(bf16[256,2048]{1,0:T(8,128)(2,1)S(1)} %copy-done, bf16[2048,256]{1,0:T(8,128)(2,1)S(1)} %copy-done.11, f32[642,256]{1,0:T(8,128)S(1)} %maximum_convert_fusion, f32[256]{0:T(256)S(1)} %bitcast.60, f32[256]{0:T(256)S(1)} %bitcast.61, f32[256]{0:T(256)S(1)} %bitcast.59, ...), kind=kOutput, calls=%fused_computation.17 | convolution fusion | flops 1349877760 | bytes 9321472 | tf_op jit(solution)/shard_map/dot_general | solution.py:84
  142.7 52.8 %all-to-all-done.1 = bf16[8,80,2048]{2,1,0:T(8,128)(2,1)} async-done(((bf16[8,80,2048]{2,1,0:T(8,128)(2,1)}), bf16[8,80,2048]{2,1,0:T(8,128)(2,1)}, u32[]{:S(2)}, u32[]{:S(2)}) %all-to-all-start.1) | async-done | bytes 2621472 | tf_op jit(solution)/shard_map/all_to_all | solution.py:116
  195.5 7.0 %gather_fusion.1 = bf16[320,2048]{1,0:T(8,128)(2,1)} fusion(bf16[640,2048]{1,0:T(8,128)(2,1)} %bitcast.17, s32[1024]{0:T(1024)S(1)} %pad_clamp_fusion), kind=kCustom, calls=%fused_computation.1 | custom fusion | bytes 2622720 | tf_op jit(solution)/shard_map/gather | solution.py:120
  202.5 3.1 %reshape.96 = bf16[160,2,2048]{2,1,0:T(2,128)(2,1)S(1)} reshape(bf16[320,2048]{1,0:T(8,128)(2,1)} %gather_fusion.1) | data formatting | bytes 2621440 | tf_op jit(solution)/shard_map/reshape | solution.py:120
  205.6 1.8 fusion.41
  207.4 2.2 %fusion.13 = bf16[160,2048]{1,0:T(8,128)(2,1)} fusion(bf16[160,1,2048]{2,1,0:T(2,128)(2,1)S(1)} %get-tuple-element.3, bf16[160,1,2048]{2,1,0:T(2,128)(2,1)S(1)} %get-tuple-element.2, f32[160]{0:T(256)S(1)} %bitcast.57, f32[160]{0:T(256)S(1)} %bitcast.56), kind=kLoop, calls=%fused_computation.26 | loop fusion | flops 1966080 | bytes 1967360 | tf_op jit(solution)/shard_map/convert_element_type | solution.py:124
  (68 shorter events, 8.2 us)
Async XLA Ops:
  7.2 128.6 %copy-start = (bf16[256,2048]{1,0:T(8,128)(2,1)S(1)}, bf16[256,2048]{1,0:T(8,128)(2,1)}, u32[]{:S(2)}) copy-start(bf16[256,2048]{1,0:T(8,128)(2,1)} %param.21) | copy-start | bytes 3145732
  7.2 4.5 %copy-start.3 = (bf16[160,2048]{1,0:T(8,128)(2,1)S(1)}, bf16[160,2048]{1,0:T(8,128)(2,1)}, u32[]{:S(2)}) copy-start(bf16[160,2048]{1,0:T(8,128)(2,1)} %param.22) | copy-start | bytes 1966084
  7.2 4.8 %copy-start.5 = (f32[2048]{0:T(1024)S(1)}, f32[2048]{0:T(1024)}, u32[]{:S(2)}) copy-start(f32[2048]{0:T(1024)} %param.23) | copy-start | bytes 24580
  7.2 79.1 %all-gather.6.cloned.1.call-start = ((), (), s32[]{:S(2)}) async-start(), calls=%async_computation.5 | async-start | bytes 5242880 | tf_op jit(solution)/shard_map/all_gather | solution.py:108
  7.9 85.6 %all-gather.4.cloned.1.call-start = ((), (), s32[]{:S(2)}) async-start(), calls=%async_computation.4 | async-start | bytes 5242880 | tf_op jit(solution)/shard_map/all_gather | solution.py:107
  19.4 66.9 %all-to-all-start = ((bf16[8,80,2048]{2,1,0:T(8,128)(2,1)}), bf16[8,80,2048]{2,1,0:T(8,128)(2,1)}, u32[]{:S(2)}, u32[]{:S(2)}) async-start(bf16[8,80,2048]{2,1,0:T(8,128)(2,1)} %bitcast.53), calls=%async_computation.1 | async-start | bytes 5242880 | tf_op jit(solution)/shard_map/all_to_all | solution.py:111
  26.7 3.2 %copy-start.9 = (bf16[2048,256]{1,0:T(8,128)(2,1)S(1)}, bf16[2048,256]{1,0:T(8,128)(2,1)}, u32[]{:S(2)}) copy-start(bf16[2048,256]{1,0:T(8,128)(2,1)} %param.18) | copy-start | bytes 3145732
  26.7 3.3 %copy-start.12 = (f32[2048]{0:T(1024)S(1)}, f32[2048]{0:T(1024)}, u32[]{:S(2)}) copy-start(f32[2048]{0:T(1024)} %param.16) | copy-start | bytes 24580
  26.7 93.3 %all-gather.8.cloned.1.call-start = ((), (), s32[]{:S(2)}) async-start(), calls=%async_computation.6 | async-start | bytes 5242880 | tf_op jit(solution)/shard_map/all_gather | solution.py:109
  27.4 2.6 %copy-start.2 = (bf16[640,2048]{1,0:T(8,128)(2,1)S(1)}, bf16[640,2048]{1,0:T(8,128)(2,1)}, u32[]{:S(2)}) copy-start(bf16[640,2048]{1,0:T(8,128)(2,1)} %param.15) | copy-start | bytes 7864324
  30.0 1.2 copy-start.10
  31.3 6.3 %copy-start.7 = (f32[3,256]{1,0:T(4,128)S(1)}, f32[3,256]{1,0:T(4,128)}, u32[]{:S(2)}) copy-start(f32[3,256]{1,0:T(4,128)} %param.20) | copy-start | bytes 9220
  32.2 15.9 %collective-permute-start = (bf16[1,256]{1,0:T(2,128)(2,1)S(1)}, bf16[1,256]{1,0:T(2,128)(2,1)S(1)}, u32[]{:S(2)}, u32[]{:S(2)}) collective-permute-start(bf16[1,256]{1,0:T(2,128)(2,1)S(1)} %get-tuple-element.4), channel_id=1, source_target_pairs={{0,4},{4,8},{8,12},{12,16},{16,20},{20,24},{24,28},{1,5},{5,9},{9,... | collective-permute-start | bytes 1544 | tf_op jit(solution)/shard_map/ppermute | solution.py:18
  36.1 11.9 %collective-permute-start.1 = (bf16[1,256]{1,0:T(2,128)(2,1)S(1)}, bf16[1,256]{1,0:T(2,128)(2,1)S(1)}, u32[]{:S(2)}, u32[]{:S(2)}) collective-permute-start(bf16[1,256]{1,0:T(2,128)(2,1)S(1)} %get-tuple-element.5), channel_id=1, source_target_pairs={{4,0},{8,4},{12,8},{16,12},{20,16},{24,20},{28,24},{5,1},{9,5},{13... | collective-permute-start | bytes 1544 | tf_op jit(solution)/shard_map/ppermute | solution.py:20
  120.0 4.3 %copy-start.1 = (bf16[1,1024,2048]{2,1,0:T(8,128)(2,1)S(1)}, bf16[1,1024,2048]{2,1,0:T(8,128)(2,1)}, u32[]{:S(2)}) copy-start(bf16[1,1024,2048]{2,1,0:T(8,128)(2,1)} %all-gather.8.cloned.1.call-done) | copy-start | bytes 12582916
  129.9 5.9 %copy-start.11 = (bf16[2048,256]{1,0:T(8,128)(2,1)S(1)}, bf16[2048,256]{1,0:T(8,128)(2,1)}, u32[]{:S(2)}) copy-start(bf16[2048,256]{1,0:T(8,128)(2,1)} %param.19) | copy-start | bytes 3145732
  129.9 65.6 %all-to-all-start.1 = ((bf16[8,80,2048]{2,1,0:T(8,128)(2,1)}), bf16[8,80,2048]{2,1,0:T(8,128)(2,1)}, u32[]{:S(2)}, u32[]{:S(2)}) async-start(bf16[8,80,2048]{2,1,0:T(8,128)(2,1)} %bitcast.54), calls=%async_computation.2 | async-start | bytes 5242880 | tf_op jit(solution)/shard_map/all_to_all | solution.py:116
  135.5 74.1 %reduce-scatter.2.cloned.1.call-start = ((), (), s32[]{:S(2)}) async-start(), calls=%async_computation.3 | async-start | bytes 3276800 | tf_op jit(solution)/shard_map/reduce_scatter | solution.py:83
  141.9 0.7 copy-start.6
  141.9 0.8 copy-start.4
  141.9 0.8 copy-start.8
Sparse Core Ops, SparseCore 0:
  9.6 37.7 all-gather.5
  48.9 34.9 all-gather.3
  85.5 34.4 all-gather.7
  142.1 34.7 reduce-scatter.1
where the time goes:
time: 217 us; the launch traced here: 216 us
  waiting for transfers between devices  122 us (56%)
  matrix products  28.8 us (13%)
  local copies, waits for them, and re-layouts  21.5 us (10%)
  starting transfers between devices  18.7 us (9%)
  between operations  14.1 us (6%)
  other arithmetic  10.8 us (5%)
    all_to_all x1, waiting for transfers between devices, on_device(): lax.all_to_all(answers.reshape(senders, items, width), 'ep', split_axis=0...  52.8 us
    all_to_all x1, waiting for transfers between devices, on_device(): lax.all_to_all(outgoing, 'ep', split_axis=0, concat_axis=0, tiled=True)  38.1 us
    all_gather x1, waiting for transfers between devices, on_device(): lax.all_gather(down_weight, 'tp', axis=1, tiled=True)  18.9 us
    ppermute x1, waiting for transfers between devices, padded_2(): lax.ppermute(tail, axis, [(i, (i + 1) % count) for i in range(ends)])  10.4 us
    dot_general x1, matrix products, expert_block_local(): first = jnp.dot(rows, gate, preferred_element_type=jnp.float32)  7.54 us
    dot_general x1, matrix products, expert_block_local(): second = jnp.dot(rows, upper, preferred_element_type=jnp.float32)  7.31 us
    all_to_all x1, starting transfers between devices, on_device(): lax.all_to_all(outgoing, 'ep', split_axis=0, concat_axis=0, tiled=True)  7.28 us
    gather x1, local copies, waits for them, and re-layouts, on_device(): pairs = answered[slots].reshape(local, 2, width)  7.03 us
  transfers between devices with their start and end apart: 8, of which 4 were waited for; matrix products, arithmetic and copies ran while one was open for 23% of the time, Pallas kernels for 0%

commit v1 on v0

--- a/solution.py
+++ b/solution.py
@@ -69,6 +69,13 @@
     up_weight,
     down_weight,
 ):
+
+    def page_connect(u_in):
+        parts_out = jnp.concatenate(
+            lax.all_to_all(jnp.stack([u_in] * lax.axis_size("tp"), 0), "tp", 0, 0), 1
+        )
+        return parts_out
+
     split = lax.axis_size("tp")
     normal_rows = normed(mixer_input, mixer_gain)
     values = jnp.dot(normal_rows, value_weight, preferred_element_type=jnp.float32)
@@ -106,7 +113,7 @@
     whole_gate, whole_up, whole_down = (
         lax.all_gather(gate_weight, "tp", axis=2, tiled=True),
         lax.all_gather(up_weight, "tp", axis=2, tiled=True),
-        lax.all_gather(down_weight, "tp", axis=1, tiled=True),
+        page_connect(down_weight),
     )
     arrived = lax.all_to_all(outgoing, "ep", split_axis=0, concat_axis=0, tiled=True)
     senders, items, _ = arrived.shape

time: 217 us -> 241 us (1.11)
  waiting for transfers between devices: 122 us -> 135 us
  matrix products: 28.8 us -> 32.4 us
  starting transfers between devices: 18.7 us -> 22 us
    all_to_all x0 -> x1, waiting for transfers between devices: none -> 21.1 us  [page_connect(): lax.all_to_all(jnp.stack([u_in] * lax.axis_size('tp'), 0), 'tp', 0, 0)]
    all_gather x1 -> x0, waiting for transfers between devices: 18.9 us -> none  [on_device(): lax.all_gather(down_weight, 'tp', axis=1, tiled=True)]
    all_to_all x1, waiting for transfers between devices: 38.1 us -> 56.5 us  [on_device(): lax.all_to_all(outgoing, 'ep', split_axis=0, concat_axis=0, tiled=True)]
    ppermute x1, waiting for transfers between devices: 10.4 us -> 0.01 us  [padded_2(): lax.ppermute(tail, axis, [(i, (i + 1) % count) for i in range(ends)])]
    all_to_all x0 -> x1, starting transfers between devices: none -> 4.97 us  [page_connect(): lax.all_to_all(jnp.stack([u_in] * lax.axis_size('tp'), 0), 'tp', 0, 0)]
    ppermute x1, waiting for transfers between devices: 0.01 us -> 3.95 us  [padded_2(): lax.ppermute(head, axis, [((i + 1) % count, i) for i in range(ends)])]
    another operation x0 -> x1, local copies, waits for them, and re-layouts: none -> 2.47 us  [page_connect(): jnp.stack([u_in] * lax.axis_size('tp'), 0)]
where the time goes in v1:
time: 241 us; the launch traced here: 240 us
  waiting for transfers between devices  135 us (56%)
  matrix products  32.4 us (13%)
  local copies, waits for them, and re-layouts  23.6 us (10%)
  starting transfers between devices  22 us (9%)
  between operations  14.1 us (6%)
  other arithmetic  12.8 us (5%)
    all_to_all x1, waiting for transfers between devices, on_device(): lax.all_to_all(outgoing, 'ep', split_axis=0, concat_axis=0, tiled=True)  56.5 us
    all_to_all x1, waiting for transfers between devices, on_device(): lax.all_to_all(answers.reshape(senders, items, width), 'ep', split_axis=0...  52.2 us
    all_to_all x1, waiting for transfers between devices, page_connect(): lax.all_to_all(jnp.stack([u_in] * lax.axis_size('tp'), 0), 'tp', 0, 0)  21.1 us
    dot_general x4, matrix products, blockwise_sum(): jnp.dot(left[:, block * width:(block + 1) * width], right[block * width:(...  8.3 us
    dot_general x1, matrix products, expert_block_local(): second = jnp.dot(rows, upper, preferred_element_type=jnp.float32)  7.37 us
    all_to_all x1, starting transfers between devices, on_device(): lax.all_to_all(outgoing, 'ep', split_axis=0, concat_axis=0, tiled=True)  7.28 us
    gather x1, local copies, waits for them, and re-layouts, on_device(): pairs = answered[slots].reshape(local, 2, width)  7.03 us
    dot_general x1, matrix products, expert_block_local(): first = jnp.dot(rows, gate, preferred_element_type=jnp.float32)  6.92 us
  transfers between devices with their start and end apart: 8, of which 4 were waited for; matrix products, arithmetic and copies ran while one was open for 23% of the time, Pallas kernels for 0%

profile of v1, /device:TPU:0, one launch (start us, length us, event | category | flops | bytes accessed | tf_op | source)
XLA Modules:
  0.0 240.1 jit_solution(1038259543088721644)
XLA Ops:
  13.8 2.9 %scatter_custom_fusion = s32[640]{0:T(1024)S(1)} fusion(s32[320]{0:T(512)S(1)} %fusion.34, s32[320]{0:T(512)S(1)} %add_select_fusion, s32[]{:T(128)} %constant.59.clone.1), kind=kCustom, calls=%fused_computation.75 | custom fusion | bytes 2564 | tf_op jit(solution)/shard_map/scatter | solution.py:109
  16.7 4.1 %gather_fusion = bf16[640,2048]{1,0:T(8,128)(2,1)} fusion(bf16[161,2048]{1,0:T(8,128)(2,1)S(1)} %concatenate.7, s32[1024]{0:T(1024)S(1)} %pad_clamp_fusion.1), kind=kCustom, calls=%fused_computation | custom fusion | bytes 5245440 | tf_op jit(solution)/shard_map/gather | solution.py:112
  20.8 7.3 %all-to-all-start = ((bf16[8,80,2048]{2,1,0:T(8,128)(2,1)}), bf16[8,80,2048]{2,1,0:T(8,128)(2,1)}, u32[]{:S(2)}, u32[]{:S(2)}) async-start(bf16[8,80,2048]{2,1,0:T(8,128)(2,1)} %bitcast.54), calls=%async_computation.1 | async-start | bytes 5242880 | tf_op jit(solution)/shard_map/all_to_all | solution.py:118
  28.9 2.3 fusion
  31.2 56.5 %all-to-all-done = bf16[8,80,2048]{2,1,0:T(8,128)(2,1)} async-done(((bf16[8,80,2048]{2,1,0:T(8,128)(2,1)}), bf16[8,80,2048]{2,1,0:T(8,128)(2,1)}, u32[]{:S(2)}, u32[]{:S(2)}) %all-to-all-start) | async-done | bytes 2621472 | tf_op jit(solution)/shard_map/all_to_all | solution.py:118
  87.7 2.5 %stack.2 = bf16[4,1,256,2048]{3,2,1,0:T(8,128)(2,1)} broadcast(bf16[256,2048]{1,0:T(8,128)(2,1)S(1)} %bitcast.56), dimensions={2,3} | broadcast | bytes 5242880 | tf_op jit(solution)/shard_map/stack | solution.py:75
  90.2 5.0 %all-to-all-start.1 = ((bf16[4,1,256,2048]{3,2,1,0:T(8,128)(2,1)}), bf16[4,1,256,2048]{3,2,1,0:T(8,128)(2,1)}, u32[]{:S(2)}, u32[]{:S(2)}) async-start(bf16[4,1,256,2048]{3,2,1,0:T(8,128)(2,1)} %stack.2), calls=%async_computation.2 | async-start | bytes 8388608 | tf_op jit(solution)/shard_map/all_to_all | solution.py:75
  95.2 2.8 %fusion.37 = f32[640,256]{1,0:T(8,128)S(1)} fusion(bf16[2048,256]{1,0:T(8,128)(2,1)S(1)} %copy-done.7, bf16[640,2048]{1,0:T(8,128)(2,1)} %param.15, f32[2048]{0:T(1024)S(1)} %copy-done.10, f32[640]{0:T(1024)S(1)} %add_rsqrt_fusion), kind=kOutput, calls=%fused_computation.84 | convolution fusion | flops 676331520 | bytes 4336128 | tf_op jit(solution)/shard_map/dot_general | solution.py:82
  99.0 3.4 %collective-permute-start = (bf16[1,256]{1,0:T(2,128)(2,1)S(1)}, bf16[1,256]{1,0:T(2,128)(2,1)S(1)}, u32[]{:S(2)}, u32[]{:S(2)}) collective-permute-start(bf16[1,256]{1,0:T(2,128)(2,1)S(1)} %get-tuple-element.4), channel_id=1, source_target_pairs={{0,4},{4,8},{8,12},{12,16},{16,20},{20,24},{24,28},{1,5},{5,9},{9,... | collective-permute-start | bytes 1544 | tf_op jit(solution)/shard_map/ppermute | solution.py:18
  103.9 4.0 %collective-permute-done.1 = bf16[1,256]{1,0:T(2,128)(2,1)S(1)} collective-permute-done((bf16[1,256]{1,0:T(2,128)(2,1)S(1)}, bf16[1,256]{1,0:T(2,128)(2,1)S(1)}, u32[]{:S(2)}, u32[]{:S(2)}) %collective-permute-start.1) | collective-permute-done | bytes 544 | tf_op jit(solution)/shard_map/ppermute | solution.py:20
  107.9 7.4 %fusion.3 = f32[640,1024]{1,0:T(8,128)} fusion(bf16[640,2048]{1,0:T(8,128)(2,1)} %bitcast.9, bf16[1,2048,1024]{2,1,0:T(8,128)(2,1)} %all-gather.5.cloned.1.call-done), kind=kOutput, calls=%fused_computation.9 | convolution fusion | flops 2684354560 | bytes 9437184 | tf_op jit(solution)/shard_map/dot_general | solution.py:137
  115.3 6.9 %multiply_convert_fusion = bf16[640,1024]{1,0:T(8,128)(2,1)S(1)} fusion(f32[640,1024]{1,0:T(8,128)} %fusion.3, bf16[640,2048]{1,0:T(8,128)(2,1)} %bitcast.9, bf16[1,2048,1024]{2,1,0:T(8,128)(2,1)} %all-gather.3.cloned.1.call-done), kind=kOutput, calls=%fused_computation.18 | convolution fusion | flops 2688286720 | bytes 10747904 | tf_op jit(solution)/shard_map/dot_general | solution.py:136
  122.2 21.1 %all-to-all-done.1 = bf16[4,1,256,2048]{3,2,1,0:T(8,128)(2,1)} async-done(((bf16[4,1,256,2048]{3,2,1,0:T(8,128)(2,1)}), bf16[4,1,256,2048]{3,2,1,0:T(8,128)(2,1)}, u32[]{:S(2)}, u32[]{:S(2)}) %all-to-all-start.1) | async-done | bytes 4194336 | tf_op jit(solution)/shard_map/all_to_all | solution.py:75
  143.3 2.1 convolution_convert_fusion.3
  145.4 2.1 convolution_convert_fusion.2
  147.5 2.1 convolution_convert_fusion.1
  149.6 2.1 convolution_convert_fusion
  151.7 3.8 %add_convert_fusion = bf16[640,2048]{1,0:T(8,128)(2,1)} fusion(bf16[640,2048]{1,0:T(8,128)(2,1)S(1)} %convolution_convert_fusion, bf16[640,2048]{1,0:T(8,128)(2,1)S(1)} %convolution_convert_fusion.1, bf16[640,2048]{1,0:T(8,128)(2,1)S(1)} %convolution_convert_fusion.2, bf16[640,2048]{1,0:T(8,128)(2,1)S(1)} %convolution_convert_fusion.3), kind=kLoop, calls=%fused_computation.8 | loop fusion | flops 10485760 | bytes 13107200 | tf_op jit(solution)/shard_map/convert_element_type | solution.py:44
  155.5 4.5 %all-to-all-start.2 = ((bf16[8,80,2048]{2,1,0:T(8,128)(2,1)}), bf16[8,80,2048]{2,1,0:T(8,128)(2,1)}, u32[]{:S(2)}, u32[]{:S(2)}) async-start(bf16[8,80,2048]{2,1,0:T(8,128)(2,1)} %bitcast.55), calls=%async_computation.3 | async-start | bytes 5242880 | tf_op jit(solution)/shard_map/all_to_all | solution.py:123
  160.3 6.1 %convolution_convert_fusion.4 = bf16[640,2048]{1,0:T(8,128)(2,1)} fusion(bf16[256,2048]{1,0:T(8,128)(2,1)S(1)} %copy-done, bf16[2048,256]{1,0:T(8,128)(2,1)S(1)} %copy-done.9, f32[642,256]{1,0:T(8,128)S(1)} %maximum_convert_fusion, f32[256]{0:T(256)S(1)} %bitcast.62, f32[256]{0:T(256)S(1)} %bitcast.63, f32[256]{0:T(256)S(1)} %bitcast.61, ...), kind=kOutput, calls=%fused_computation.17 | convolution fusion | flops 1349877760 | bytes 9321472 | tf_op jit(solution)/shard_map/dot_general | solution.py:91
  167.3 52.2 %all-to-all-done.2 = bf16[8,80,2048]{2,1,0:T(8,128)(2,1)} async-done(((bf16[8,80,2048]{2,1,0:T(8,128)(2,1)}), bf16[8,80,2048]{2,1,0:T(8,128)(2,1)}, u32[]{:S(2)}, u32[]{:S(2)}) %all-to-all-start.2) | async-done | bytes 2621472 | tf_op jit(solution)/shard_map/all_to_all | solution.py:123
  219.5 7.0 %gather_fusion.1 = bf16[320,2048]{1,0:T(8,128)(2,1)} fusion(bf16[640,2048]{1,0:T(8,128)(2,1)} %bitcast.18, s32[1024]{0:T(1024)S(1)} %pad_clamp_fusion), kind=kCustom, calls=%fused_computation.1 | custom fusion | bytes 2622720 | tf_op jit(solution)/shard_map/gather | solution.py:127
  226.5 3.1 %reshape.99 = bf16[160,2,2048]{2,1,0:T(2,128)(2,1)S(1)} reshape(bf16[320,2048]{1,0:T(8,128)(2,1)} %gather_fusion.1) | data formatting | bytes 2621440 | tf_op jit(solution)/shard_map/reshape | solution.py:127
  231.4 2.2 fusion.13
  (64 shorter events, 12.7 us)
Async XLA Ops:
  7.2 153.2 %copy-start = (bf16[256,2048]{1,0:T(8,128)(2,1)S(1)}, bf16[256,2048]{1,0:T(8,128)(2,1)}, u32[]{:S(2)}) copy-start(bf16[256,2048]{1,0:T(8,128)(2,1)} %param.21) | copy-start | bytes 3145732
  7.2 100.7 %all-gather.5.cloned.1.call-start = ((), (), s32[]{:S(2)}) async-start(), calls=%async_computation.6 | async-start | bytes 5242880 | tf_op jit(solution)/shard_map/all_gather | solution.py:115
  20.8 66.9 %all-to-all-start = ((bf16[8,80,2048]{2,1,0:T(8,128)(2,1)}), bf16[8,80,2048]{2,1,0:T(8,128)(2,1)}, u32[]{:S(2)}, u32[]{:S(2)}) async-start(bf16[8,80,2048]{2,1,0:T(8,128)(2,1)} %bitcast.54), calls=%async_computation.1 | async-start | bytes 5242880 | tf_op jit(solution)/shard_map/all_to_all | solution.py:118
  28.1 59.6 %copy-start.2 = (bf16[1,256,2048]{2,1,0:T(8,128)(2,1)S(1)}, bf16[1,256,2048]{2,1,0:T(8,128)(2,1)}, u32[]{:S(2)}) copy-start(bf16[1,256,2048]{2,1,0:T(8,128)(2,1)} %param.29) | copy-start | bytes 3145732
  28.1 87.2 %all-gather.3.cloned.1.call-start = ((), (), s32[]{:S(2)}) async-start(), calls=%async_computation.5 | async-start | bytes 5242880 | tf_op jit(solution)/shard_map/all_gather | solution.py:114
  90.1 5.0 %copy-start.7 = (bf16[2048,256]{1,0:T(8,128)(2,1)S(1)}, bf16[2048,256]{1,0:T(8,128)(2,1)}, u32[]{:S(2)}) copy-start(bf16[2048,256]{1,0:T(8,128)(2,1)} %param.18) | copy-start | bytes 3145732
  90.2 5.0 %copy-start.10 = (f32[2048]{0:T(1024)S(1)}, f32[2048]{0:T(1024)}, u32[]{:S(2)}) copy-start(f32[2048]{0:T(1024)} %param.16) | copy-start | bytes 24580
  90.2 53.2 %all-to-all-start.1 = ((bf16[4,1,256,2048]{3,2,1,0:T(8,128)(2,1)}), bf16[4,1,256,2048]{3,2,1,0:T(8,128)(2,1)}, u32[]{:S(2)}, u32[]{:S(2)}) async-start(bf16[4,1,256,2048]{3,2,1,0:T(8,128)(2,1)} %stack.2), calls=%async_computation.2 | async-start | bytes 8388608 | tf_op jit(solution)/shard_map/all_to_all | solution.py:75
  95.2 2.8 %copy-start.1 = (bf16[640,2048]{1,0:T(8,128)(2,1)S(1)}, bf16[640,2048]{1,0:T(8,128)(2,1)}, u32[]{:S(2)}) copy-start(bf16[640,2048]{1,0:T(8,128)(2,1)} %param.15) | copy-start | bytes 7864324
  95.2 2.8 %copy-start.8 = (bf16[2048,256]{1,0:T(8,128)(2,1)S(1)}, bf16[2048,256]{1,0:T(8,128)(2,1)}, u32[]{:S(2)}) copy-start(bf16[2048,256]{1,0:T(8,128)(2,1)} %param.17) | copy-start | bytes 3145732
  98.0 5.8 %copy-start.5 = (f32[3,256]{1,0:T(4,128)S(1)}, f32[3,256]{1,0:T(4,128)}, u32[]{:S(2)}) copy-start(f32[3,256]{1,0:T(4,128)} %param.20) | copy-start | bytes 9220
  99.0 4.9 %collective-permute-start = (bf16[1,256]{1,0:T(2,128)(2,1)S(1)}, bf16[1,256]{1,0:T(2,128)(2,1)S(1)}, u32[]{:S(2)}, u32[]{:S(2)}) collective-permute-start(bf16[1,256]{1,0:T(2,128)(2,1)S(1)} %get-tuple-element.4), channel_id=1, source_target_pairs={{0,4},{4,8},{8,12},{12,16},{16,20},{20,24},{24,28},{1,5},{5,9},{9,... | collective-permute-start | bytes 1544 | tf_op jit(solution)/shard_map/ppermute | solution.py:18
  102.3 5.5 %collective-permute-start.1 = (bf16[1,256]{1,0:T(2,128)(2,1)S(1)}, bf16[1,256]{1,0:T(2,128)(2,1)S(1)}, u32[]{:S(2)}, u32[]{:S(2)}) collective-permute-start(bf16[1,256]{1,0:T(2,128)(2,1)S(1)} %get-tuple-element.5), channel_id=1, source_target_pairs={{4,0},{8,4},{12,8},{16,12},{20,16},{24,20},{28,24},{5,1},{9,5},{13... | collective-permute-start | bytes 1544 | tf_op jit(solution)/shard_map/ppermute | solution.py:20
  155.5 4.8 %copy-start.9 = (bf16[2048,256]{1,0:T(8,128)(2,1)S(1)}, bf16[2048,256]{1,0:T(8,128)(2,1)}, u32[]{:S(2)}) copy-start(bf16[2048,256]{1,0:T(8,128)(2,1)} %param.19) | copy-start | bytes 3145732
  155.5 64.0 %all-to-all-start.2 = ((bf16[8,80,2048]{2,1,0:T(8,128)(2,1)}), bf16[8,80,2048]{2,1,0:T(8,128)(2,1)}, u32[]{:S(2)}, u32[]{:S(2)}) async-start(bf16[8,80,2048]{2,1,0:T(8,128)(2,1)} %bitcast.55), calls=%async_computation.3 | async-start | bytes 5242880 | tf_op jit(solution)/shard_map/all_to_all | solution.py:123
  160.0 73.6 %reduce-scatter.2.cloned.1.call-start = ((), (), s32[]{:S(2)}) async-start(), calls=%async_computation.4 | async-start | bytes 3276800 | tf_op jit(solution)/shard_map/reduce_scatter | solution.py:90
  166.5 0.7 copy-start.4
  166.5 0.8 copy-start.3
  166.5 0.8 copy-start.6
Sparse Core Ops, SparseCore 0:
  9.5 37.7 all-gather.4
  48.8 34.9 all-gather.2
  166.6 34.6 reduce-scatter.1
